TPU v7x, 32 devices: a whole 2x2x4 slice. The times are simulated.
32 devices in a mesh: ep: 8 (over z, y), tp: 4 (over x, core).
Axes of the slice: x: 2, y: 2, z: 4, core: 2. Of those that a mesh axis runs over, the one named last changes fastest.
Arguments:
- tokens: bfloat16 [256, 2048], P('ep', 'tp'), may hold values from -33 to 33
- previous: bfloat16 [256, 2048], P('ep', 'tp'), may hold values from -6 to 6
- first_norm_gain: float32 [2048], replicated, may hold values from 0.1 to 1.9
- token_shift_share: float32 [5, 2048], replicated, may hold values from 0 to 1
- receptance_weight: bfloat16 [2048, 1024], P(None, 'tp'), may hold values from -0.125 to 0.125
- key_weight: bfloat16 [2048, 1024], P(None, 'tp'), may hold values from -0.125 to 0.125
- value_weight: bfloat16 [2048, 1024], P(None, 'tp'), may hold values from -0.125 to 0.125
- decay_down_map: bfloat16 [2048, 128], replicated, may hold values from -0.125 to 0.125
- decay_up_map: bfloat16 [128, 1024], replicated, may hold values from -0.5 to 0.5
- decay_offset: float32 [1024], P('tp'), may hold values from -4 to 1
- strength_down_map: bfloat16 [2048, 128], replicated, may hold values from -0.125 to 0.125
- strength_up_map: bfloat16 [128, 1024], replicated, may hold values from -0.5 to 0.5
- removal_key_scale: float32 [1024], P('tp'), may hold values from 0.3 to 3
- key_damping: float32 [1024], P('tp'), may hold values from 0.1 to 1.9
- self_term_weight: float32 [16, 64], P('tp'), may hold values from -0.6 to 0.6
- head_norm_gain: float32 [1024], P('tp'), may hold values from 0.1 to 1.9
- output_weight: bfloat16 [1024, 2048], P('tp'), may hold values from -0.1875 to 0.1875
- state: float32 [256, 16, 64, 64], P('ep', 'tp'), may hold values from -6 to 6
- second_norm_gain: float32 [2048], replicated, may hold values from 0.1 to 1.9
- routes: int32 [256, 4], P('ep'), may hold values from 0 to 7, all different within a row; in each aligned block of 32 rows (0 to 31, 32 to 63, ...) at most 24 rows name the same one
- chosen_expert_weight: float32 [256, 4], P('ep'), may hold values from 0.1 to 1
- expert_gate_weight: bfloat16 [8, 2048, 1024], P('ep', None, 'tp'), may hold values from -0.5 to 0.5
- expert_up_weight: bfloat16 [8, 2048, 1024], P('ep', None, 'tp'), may hold values from -0.5 to 0.5
- expert_down_weight: bfloat16 [8, 1024, 2048], P('ep', 'tp'), may hold values from -0.046875 to 0.046875
Outputs:
- layer_out: bfloat16 [256, 2048], P('ep', 'tp')
- new_state: float32 [256, 16, 64, 64], P('ep', 'tp')
Inputs may be any that keep to these rules, and one draw needn't show every extreme that they name: `routes`: each row names 4 different experts. Among the rows of one index of ep no expert is named by more than 24 rows, and in every draw some expert is named by exactly 24 rows of some index of ep.
All inputs are finite; a program needn't handle non-finite values.
Results may differ from a plain program's by a relative error of at most 0.015.
Values may be sent and summed in bfloat16 or wider, within the bound.
A program may use at most 64 MiB of HBM per device.

v0:
```python
import jax
import jax.numpy as jnp
from jax import lax
from jax.sharding import PartitionSpec as P

NORM_EPS = 1e-06
GROUP_EPS = 0.00064
KEY_EPS = 1e-06
GATE_LIMIT = 7.0
GATE_SLOPE = 1.702


def row_rescale(values, gain):
    return values * lax.rsqrt(jnp.mean(values * values, axis=-1, keepdims=True) + NORM_EPS) * gain


def head_combiner(
    present_rows,
    prior_rows,
    first_norm_gain,
    token_shift_share,
    receptance_weight,
    key_weight,
    value_weight,
    decay_down_map,
    decay_up_map,
    decay_offset,
    strength_down_map,
    strength_up_map,
    removal_key_scale,
    key_damping,
    self_term_weight,
    head_norm_gain,
    state,
):
    sequence_count = present_rows.shape[0]
    head_number = state.shape[1]
    head_extent = state.shape[2]
    normed = row_rescale(present_rows.astype(jnp.float32), first_norm_gain)
    before = prior_rows.astype(jnp.float32)

    def shifted(role):
        return (normed + (before - normed) * token_shift_share[role]).astype(jnp.bfloat16)

    def project(inputs, weight):
        return jnp.dot(inputs, weight, preferred_element_type=jnp.float32)

    def by_heads(values):
        return values.reshape(sequence_count, head_number, head_extent)

    receptance_rows = by_heads(project(shifted(0), receptance_weight))
    key_rows = by_heads(project(shifted(1), key_weight))
    value_matrix = by_heads(project(shifted(2), value_weight))
    decay_low = jnp.tanh(project(shifted(3), decay_down_map)).astype(jnp.bfloat16)
    decay_pre = decay_offset + project(decay_low, decay_up_map)
    decay = by_heads(jnp.exp(-jnp.exp(-jax.nn.softplus(-decay_pre) - 0.5)))
    alpha_low = project(shifted(4), strength_down_map).astype(jnp.bfloat16)
    alpha = by_heads(jax.nn.sigmoid(project(alpha_low, strength_up_map)))
    removal = key_rows * removal_key_scale.reshape(head_number, head_extent)
    removal = removal * lax.rsqrt(jnp.sum(removal * removal, axis=-1, keepdims=True) + KEY_EPS)
    blended_rows = key_rows * (1.0 + (alpha - 1.0) * key_damping.reshape(head_number, head_extent))
    highest = lax.Precision.HIGHEST
    along = jnp.einsum("shij,shj->shi", state, removal, precision=highest)
    new_state = (
        state * decay[:, :, None, :]
        - along[..., None] * (removal * alpha)[:, :, None, :]
        + value_matrix[..., None] * blended_rows[:, :, None, :]
    )
    readout = jnp.einsum("shij,shj->shi", new_state, receptance_rows, precision=highest)
    centered = readout - jnp.mean(readout, axis=-1, keepdims=True)
    variance = jnp.mean(centered * centered, axis=-1, keepdims=True)
    heads_normalised = (
        centered
        * lax.rsqrt(variance + GROUP_EPS)
        * head_norm_gain.reshape(head_number, head_extent)
    )
    self_term = (
        jnp.sum(receptance_rows * blended_rows * self_term_weight, axis=-1, keepdims=True)
        * value_matrix
    )
    mixed_inputs = (
        (heads_normalised + self_term)
        .reshape(sequence_count, head_number * head_extent)
        .astype(jnp.bfloat16)
    )
    return (mixed_inputs, new_state)


def shards(
    tokens,
    previous,
    first_norm_gain,
    token_shift_share,
    receptance_weight,
    key_weight,
    value_weight,
    decay_down_map,
    decay_up_map,
    decay_offset,
    strength_down_map,
    strength_up_map,
    removal_key_scale,
    key_damping,
    self_term_weight,
    head_norm_gain,
    output_weight,
    state,
    second_norm_gain,
    routes,
    chosen_expert_weight,
    expert_gate_weight,
    expert_up_weight,
    expert_down_weight,
):
    present_rows, prior_rows = (
        lax.all_gather(tokens, "tp", axis=1, tiled=True),
        lax.all_gather(previous, "tp", axis=1, tiled=True),
    )
    head_columns = receptance_weight.shape[1]
    head_start = lax.axis_index("tp") * head_columns
    decay_own = lax.dynamic_slice_in_dim(decay_up_map, head_start, head_columns, 1)
    alpha_own = lax.dynamic_slice_in_dim(strength_up_map, head_start, head_columns, 1)
    mixed_inputs, new_state = head_combiner(
        present_rows,
        prior_rows,
        first_norm_gain,
        token_shift_share,
        receptance_weight,
        key_weight,
        value_weight,
        decay_down_map,
        decay_own,
        decay_offset,
        strength_down_map,
        alpha_own,
        removal_key_scale,
        key_damping,
        self_term_weight,
        head_norm_gain,
        state,
    )
    head_terms = jnp.dot(mixed_inputs, output_weight, preferred_element_type=jnp.float32)
    own_columns = tokens.shape[1]
    column_start = lax.axis_index("tp") * own_columns
    residual = present_rows.astype(jnp.float32) + lax.psum(
        head_terms.astype(jnp.bfloat16), "tp"
    ).astype(jnp.float32)
    expert_rows = row_rescale(residual, second_norm_gain).astype(jnp.bfloat16)
    residual_own = lax.dynamic_slice_in_dim(residual, column_start, own_columns, 1)
    normed_own = lax.dynamic_slice_in_dim(expert_rows, column_start, own_columns, 1)
    sequences, choices_per = routes.shape
    experts = expert_gate_weight.shape[0] * lax.axis_size("ep")
    capacity = max(2, 3 * sequences * choices_per // (2 * experts))
    flattened = routes.reshape(-1)
    onehot = (flattened[:, None] == jnp.arange(experts, dtype=jnp.int32)[None, :]).astype(jnp.int32)
    ranking = jnp.sum((jnp.cumsum(onehot, axis=0) - onehot) * onehot, axis=1)
    slot_index = flattened * capacity + ranking
    placing = jnp.arange(experts * capacity, dtype=jnp.int32)[:, None] == slot_index[None, :]
    dispatch = jnp.sum(
        placing.reshape(experts * capacity, sequences, choices_per).astype(jnp.int32), axis=2
    ).astype(jnp.bfloat16)
    outgoing = jnp.dot(dispatch, normed_own, preferred_element_type=jnp.float32).astype(
        jnp.bfloat16
    )
    outgoing = outgoing.reshape(experts, capacity, -1)
    arrived = lax.all_gather(
        lax.all_to_all(outgoing, "ep", split_axis=0, concat_axis=0, tiled=True),
        "tp",
        axis=2,
        tiled=True,
    )
    sources, slot_count, feature_count = arrived.shape
    expert_input = arrived.reshape(sources * slot_count, feature_count)
    gate_pre = jnp.minimum(
        jnp.dot(expert_input, expert_gate_weight[0], preferred_element_type=jnp.float32), GATE_LIMIT
    )
    up_pre = jnp.clip(
        jnp.dot(expert_input, expert_up_weight[0], preferred_element_type=jnp.float32),
        -GATE_LIMIT,
        GATE_LIMIT,
    )
    activation = ((up_pre + 1.0) * gate_pre * jax.nn.sigmoid(GATE_SLOPE * gate_pre)).astype(
        jnp.bfloat16
    )
    down_terms = jnp.dot(activation, expert_down_weight[0], preferred_element_type=jnp.float32)
    down_terms = down_terms.reshape(sources, slot_count, -1)
    shares = lax.psum_scatter(
        down_terms.astype(jnp.bfloat16), "tp", scatter_dimension=2, tiled=True
    )
    returned = lax.all_to_all(shares, "ep", split_axis=0, concat_axis=0, tiled=True)
    returned_rows = returned.reshape(experts * capacity, -1)
    picked = jnp.take(returned_rows, slot_index, axis=0).astype(jnp.float32)
    weighted = jnp.sum(
        picked.reshape(sequences, choices_per, -1) * chosen_expert_weight[:, :, None], axis=1
    )
    layer_out = (residual_own + weighted).astype(jnp.bfloat16)
    return (layer_out, new_state)


def solution(mesh):
    in_specs = (
        P("ep", "tp"),
        P("ep", "tp"),
        P(),
        P(),
        P(None, "tp"),
        P(None, "tp"),
        P(None, "tp"),
        P(),
        P(),
        P("tp"),
        P(),
        P(),
        P("tp"),
        P("tp"),
        P("tp", None),
        P("tp"),
        P("tp", None),
        P("ep", "tp", None, None),
        P(),
        P("ep", None),
        P("ep", None),
        P("ep", None, "tp"),
        P("ep", None, "tp"),
        P("ep", "tp", None),
    )
    out_specs = (P("ep", "tp"), P("ep", "tp", None, None))
    return jax.shard_map(shards, mesh=mesh, in_specs=in_specs, out_specs=out_specs, check_vma=False)
```

profile of v0, /device:TPU:0, one launch (start us, length us, event | category | flops | bytes accessed | tf_op | source)
XLA Modules:
  0.0 153.4 jit_solution(18078987325772897809)
XLA Ops:
  7.3 6.9 %all_gather.9 = bf16[32,2048]{1,0:T(8,128)(2,1)S(1)} all-gather(bf16[32,512]{1,0:T(8,128)(2,1)} %param.24), channel_id=1, replica_groups=mesh['ep'=8,'tp'=4] {'tp'}, dimensions={1}, use_global_device_ids=true | all-gather | bytes 163840 | tf_op jit(solution)/shard_map/all_gather | solution.py:116
  14.3 5.8 %all_gather.10 = bf16[32,2048]{1,0:T(8,128)(2,1)S(1)} all-gather(bf16[32,512]{1,0:T(8,128)(2,1)} %param.25), channel_id=1, replica_groups=mesh['ep'=8,'tp'=4] {'tp'}, dimensions={1}, use_global_device_ids=true | all-gather | bytes 163840 | tf_op jit(solution)/shard_map/all_gather | solution.py:117
  20.1 1.1 fusion.83
  21.2 1.6 %fusion.29 = f32[32,256]{1,0:T(8,128)S(1)} fusion(bf16[2048,256]{1,0:T(8,128)(2,1)} %param.28, bf16[32,2048]{1,0:T(8,128)(2,1)S(1)} %all_gather.9, bf16[32,2048]{1,0:T(8,128)(2,1)S(1)} %all_gather.10, f32[2048]{0:T(1024)S(1)} %bitcast.60, f32[2048]{0:T(1024)} %param.26, f32[32]{0:T(128)S(1)} %add_rsqrt_fusion.3), kind=kOutput, calls=%fused_computation.45 | convolution fusion | flops 34078720 | bytes 1360000 | tf_op jit(solution)/shard_map/dot_general | solution.py:46
  22.8 0.7 reshape.161
  23.5 1.4 fusion.10
  25.1 1.6 %fusion.35 = f32[32,256]{1,0:T(8,128)S(1)} fusion(bf16[2048,256]{1,0:T(8,128)(2,1)} %param.29, bf16[32,2048]{1,0:T(8,128)(2,1)S(1)} %all_gather.9, bf16[32,2048]{1,0:T(8,128)(2,1)S(1)} %all_gather.10, f32[2048]{0:T(1024)S(1)} %bitcast.59, f32[2048]{0:T(1024)} %param.26, f32[32]{0:T(128)S(1)} %add_rsqrt_fusion.3), kind=kOutput, calls=%fused_computation.47 | convolution fusion | flops 34078720 | bytes 1360000 | tf_op jit(solution)/shard_map/dot_general | solution.py:46
  27.1 1.3 fusion.67
  28.5 0.3 fusion.31
  29.0 8.5 %fusion.84 = f32[32,4,1,64]{3,2,1,0:T(1,128)S(1)} fusion(f32[32,4,64,1]{2,3,1,0:T(1,128)S(1)} %bitcast.56, f32[32,4,64,64]{3,2,1,0:T(8,128)} %param.41), kind=kOutput, calls=%fused_computation.105 | convolution fusion | flops 6291456 | bytes 2162688 | tf_op jit(solution)/shard_map/shij,shj->shi/dot_general | solution.py:63
  37.5 2.8 %multiply_add_fusion = f32[32,4,64,64]{3,2,1,0:T(8,128)S(1)} fusion(f32[32,4,64,64]{3,2,1,0:T(8,128)S(1)} %copy-done.1, f32[32,4,64]{2,1,0:T(4,128)S(1)} %get-tuple-element.8, f32[32,4,64]{2,1,0:T(4,128)S(1)} %mul.306, f32[32,4,64]{2,1,0:T(4,128)S(1)} %get-tuple-element.4, f32[32,4,64]{2,1,0:T(4,128)S(1)} %bitcast.54, f32[32,4,64]{2,1,0:T(4,128)S(1)} %mul.284), kind=kLoop, calls=%fused_computation.2 | loop fusion | flops 2621440 | bytes 4358144 | tf_op jit(solution)/shard_map/add | solution.py:65
  40.4 2.0 %copy-done.2 = f32[32,4,64,64]{3,2,1,0:T(8,128)} copy-done((f32[32,4,64,64]{3,2,1,0:T(8,128)}, f32[32,4,64,64]{3,2,1,0:T(8,128)S(1)}, u32[]{:S(2)}) %copy-start.2) | copy-done | bytes 2097176
  42.3 6.6 %fusion.85 = f32[32,4,1,64]{3,2,1,0:T(1,128)S(1)} fusion(f32[32,4,64,64]{3,2,1,0:T(8,128)S(1)} %multiply_add_fusion, f32[32,4,64,1]{2,3,1,0:T(1,128)S(1)} %bitcast.55), kind=kOutput, calls=%fused_computation.106 | convolution fusion | flops 6291456 | bytes 2162688 | tf_op jit(solution)/shard_map/shij,shj->shi/dot_general | solution.py:69
  49.1 0.2 multiply_reduce_fusion.2
  49.2 0.6 add_rsqrt_fusion
  49.9 1.4 fusion.7
  51.4 0.9 convolution_convert_fusion.1
  53.3 0.8 dynamic-slice
  54.2 31.7 %all-reduce.2.cloned.1.call-done = bf16[32,2048]{1,0:T(8,128)(2,1)} async-done(((bf16[32,2048]{1,0:T(8,128)(2,1)}), bf16[32,2048]{1,0:T(8,128)(2,1)}) %all-reduce.2.cloned.1.call-update) | async-done | bytes 131088 | tf_op jit(solution)/shard_map/psum | solution.py:145
  85.8 1.1 multiply_reduce_fusion.1
  87.0 0.3 convolution_convert_fusion.2
  87.3 13.1 %all_to_all.10 = bf16[8,24,512]{2,1,0:T(8,128)(2,1)S(1)} all-to-all(bf16[8,24,512]{2,1,0:T(8,128)(2,1)S(1)} %bitcast.50), channel_id=1, replica_groups=mesh['ep'=8,'tp'=4] {'ep'}, dimensions={0} | all-to-all | bytes 393216 | tf_op jit(solution)/shard_map/all_to_all | solution.py:167
  100.3 7.6 %all_gather.11 = bf16[8,24,2048]{2,1,0:T(8,128)(2,1)S(1)} all-gather(bf16[8,24,512]{2,1,0:T(8,128)(2,1)S(1)} %all_to_all.10), channel_id=1, replica_groups=mesh['ep'=8,'tp'=4] {'tp'}, dimensions={2}, use_global_device_ids=true | all-gather | bytes 983040 | tf_op jit(solution)/shard_map/all_gather | solution.py:166
  107.9 0.4 convolution_minimum_fusion
  108.3 0.4 fusion.4
  108.7 1.3 convolution_convert_fusion
  110.0 21.4 %reduce-scatter.2.cloned.1.call-done = bf16[8,24,512]{2,1,0:T(8,128)(2,1)} async-done(((bf16[8,24,2048]{2,1,0:T(8,128)(2,1)}), bf16[8,24,512]{2,1,0:T(8,128)(2,1)}) %reduce-scatter.2.cloned.1.call-update) | async-done | bytes 196624 | tf_op jit(solution)/shard_map/reduce_scatter | solution.py:187
  131.5 5.5 %all-to-all-start.1 = ((bf16[8,24,512]{2,1,0:T(8,128)(2,1)}), bf16[8,24,512]{2,1,0:T(8,128)(2,1)S(1)}, u32[]{:S(2)}, u32[]{:S(2)}) async-start(bf16[8,24,512]{2,1,0:T(8,128)(2,1)} %reduce-scatter.2.cloned.1.call-done), calls=%async_computation.2 | async-start | bytes 393216 | tf_op jit(solution)/shard_map/all_to_all | solution.py:190
  137.4 7.4 %all-to-all-done.1 = bf16[8,24,512]{2,1,0:T(8,128)(2,1)S(1)} async-done(((bf16[8,24,512]{2,1,0:T(8,128)(2,1)}), bf16[8,24,512]{2,1,0:T(8,128)(2,1)S(1)}, u32[]{:S(2)}, u32[]{:S(2)}) %all-to-all-start.1) | async-done | bytes 196640 | tf_op jit(solution)/shard_map/all_to_all | solution.py:190
  144.8 0.8 gather_fusion
  145.7 0.3 multiply_reduce_fusion
  145.9 0.6 add_convert_fusion
  (69 shorter events, 2.8 us)
Async XLA Ops:
  7.2 101.6 %copy-start = (bf16[1,256,2048]{2,1,0:T(8,128)(2,1)S(1)}, bf16[1,256,2048]{2,1,0:T(8,128)(2,1)}, u32[]{:S(2)}) copy-start(bf16[1,256,2048]{2,1,0:T(8,128)(2,1)} %param.47) | copy-start | bytes 3145732
  7.2 19.9 %copy-start.6 = (f32[2048]{0:T(1024)S(1)}, f32[2048]{0:T(1024)}, u32[]{:S(2)}) copy-start(f32[2048]{0:T(1024)} %param.26) | copy-start | bytes 24580
  7.2 19.6 %copy-start.9 = (f32[256]{0:T(256)S(1)}, f32[256]{0:T(256)}, u32[]{:S(2)}) copy-start(f32[256]{0:T(256)} %param.36) | copy-start | bytes 3076
  7.2 19.8 %copy-start.10 = (f32[256]{0:T(256)S(1)}, f32[256]{0:T(256)}, u32[]{:S(2)}) copy-start(f32[256]{0:T(256)} %param.37) | copy-start | bytes 3076
  7.2 19.9 %copy-start.13 = (bf16[2048,128]{1,0:T(8,128)(2,1)S(1)}, bf16[2048,128]{1,0:T(8,128)(2,1)}, u32[]{:S(2)}) copy-start(bf16[2048,128]{1,0:T(8,128)(2,1)} %param.31) | copy-start | bytes 1572868
  7.2 19.8 %copy-start.15 = (f32[256]{0:T(256)S(1)}, f32[256]{0:T(256)}, u32[]{:S(2)}) copy-start(f32[256]{0:T(256)} %param.33) | copy-start | bytes 3076
  7.2 21.2 %copy-start.3 = (bf16[2048,256]{1,0:T(8,128)(2,1)S(1)}, bf16[2048,256]{1,0:T(8,128)(2,1)}, u32[]{:S(2)}) copy-start(bf16[2048,256]{1,0:T(8,128)(2,1)} %param.30) | copy-start | bytes 3145732
  7.2 78.6 %all-reduce.2.cloned.1.call-start = ((), (), s32[]{:S(2)}) async-start(), calls=%async_computation.3 | async-start | bytes 262144 | tf_op jit(solution)/shard_map/psum | solution.py:145
  28.9 8.7 %copy-start.1 = (f32[32,4,64,64]{3,2,1,0:T(8,128)S(1)}, f32[32,4,64,64]{3,2,1,0:T(8,128)}, u32[]{:S(2)}) copy-start(f32[32,4,64,64]{3,2,1,0:T(8,128)} %param.41) | copy-start | bytes 6291460
  40.3 2.0 %copy-start.2 = (f32[32,4,64,64]{3,2,1,0:T(8,128)}, f32[32,4,64,64]{3,2,1,0:T(8,128)S(1)}, u32[]{:S(2)}) copy-start(f32[32,4,64,64]{3,2,1,0:T(8,128)S(1)} %multiply_add_fusion) | copy-start | bytes 6291460
  40.3 9.5 %copy-start.11 = (f32[256]{0:T(256)S(1)}, f32[256]{0:T(256)}, u32[]{:S(2)}) copy-start(f32[256]{0:T(256)} %param.39) | copy-start | bytes 3076
  40.3 9.6 %copy-start.14 = (f32[4,64]{1,0:T(4,128)S(1)}, f32[4,64]{1,0:T(4,128)}, u32[]{:S(2)}) copy-start(f32[4,64]{1,0:T(4,128)} %param.38) | copy-start | bytes 3076
  40.4 11.1 %copy-start.4 = (bf16[256,2048]{1,0:T(8,128)(2,1)S(1)}, bf16[256,2048]{1,0:T(8,128)(2,1)}, u32[]{:S(2)}) copy-start(bf16[256,2048]{1,0:T(8,128)(2,1)} %param.40) | copy-start | bytes 3145732
  40.4 12.1 %copy-start.7 = (s32[32,4]{0,1:T(4,128)S(1)}, s32[32,4]{0,1:T(4,128)}, u32[]{:S(2)}) copy-start(s32[32,4]{0,1:T(4,128)} %param.43) | copy-start | bytes 1540
  42.3 65.6 %copy-start.5 = (bf16[1,2048,256]{2,1,0:T(8,128)(2,1)S(1)}, bf16[1,2048,256]{2,1,0:T(8,128)(2,1)}, u32[]{:S(2)}) copy-start(bf16[1,2048,256]{2,1,0:T(8,128)(2,1)} %param.45) | copy-start | bytes 3145732
  52.4 79.1 %reduce-scatter.2.cloned.1.call-start = ((), (), s32[]{:S(2)}) async-start(), calls=%async_computation.4 | async-start | bytes 983040 | tf_op jit(solution)/shard_map/reduce_scatter | solution.py:187
  85.8 22.5 %copy-start.12 = (bf16[1,2048,256]{2,1,0:T(8,128)(2,1)S(1)}, bf16[1,2048,256]{2,1,0:T(8,128)(2,1)}, u32[]{:S(2)}) copy-start(bf16[1,2048,256]{2,1,0:T(8,128)(2,1)} %param.46) | copy-start | bytes 3145732
  107.9 29.4 %copy-start.8 = (f32[32,4]{0,1:T(4,128)S(1)}, f32[32,4]{0,1:T(4,128)}, u32[]{:S(2)}) copy-start(f32[32,4]{0,1:T(4,128)} %param.44) | copy-start | bytes 1540
  131.5 13.3 %all-to-all-start.1 = ((bf16[8,24,512]{2,1,0:T(8,128)(2,1)}), bf16[8,24,512]{2,1,0:T(8,128)(2,1)S(1)}, u32[]{:S(2)}, u32[]{:S(2)}) async-start(bf16[8,24,512]{2,1,0:T(8,128)(2,1)} %reduce-scatter.2.cloned.1.call-done), calls=%async_computation.2 | async-start | bytes 393216 | tf_op jit(solution)/shard_map/all_to_all | solution.py:190
Sparse Core Ops, SparseCore 0:
  52.5 33.2 all-reduce.1
  110.1 21.2 reduce-scatter.1
where the time goes:
time: 154 us; the launch traced here: 153 us
  waiting for transfers between devices  60.5 us (39%)
  blocking collectives  33.3 us (22%)
  matrix products  24.5 us (16%)
  between operations  14.4 us (9%)
  other arithmetic  7.99 us (5%)
  local copies, waits for them, and re-layouts  7.04 us (5%)
  starting transfers between devices  5.62 us (4%)
    psum x1, waiting for transfers between devices, shards(): lax.psum(head_terms.astype(jnp.bfloat16), 'tp').astype(jnp.float32)  31.7 us
    reduce_scatter x1, waiting for transfers between devices, shards(): lax.psum_scatter(down_terms.astype(jnp.bfloat16), 'tp', scatter_dimension...  21.4 us
    all_to_all x1, blocking collectives, shards(): lax.all_to_all(outgoing, 'ep', split_axis=0, concat_axis=0, tiled=True)  13.1 us
    dot_general x1, matrix products, head_combiner(): along = jnp.einsum('shij,shj->shi', state, removal, precision=highest)  8.53 us
    all_gather x1, blocking collectives, shards(): lax.all_gather(lax.all_to_all(outgoing, 'ep', split_axis=0, concat_axis=0...  7.59 us
    all_to_all x1, waiting for transfers between devices, shards(): lax.all_to_all(shares, 'ep', split_axis=0, concat_axis=0, tiled=True)  7.37 us
    all_gather x1, blocking collectives, shards(): lax.all_gather(tokens, 'tp', axis=1, tiled=True)  6.85 us
    dot_general x1, matrix products, head_combiner(): jnp.einsum('shij,shj->shi', new_state, receptance_rows, precision=highest)  6.58 us
  transfers between devices with their start and end apart: 3, of which 3 were waited for; matrix products, arithmetic and copies ran while one was open for 1% of the time, Pallas kernels for 0%

commit v1 on v0

--- a/solution.py
+++ b/solution.py
@@ -1,3 +1,4 @@
+import functools
 import jax
 import jax.numpy as jnp
 from jax import lax
@@ -8,6 +9,14 @@
 KEY_EPS = 1e-06
 GATE_LIMIT = 7.0
 GATE_SLOPE = 1.702
+
+
+def deliver_task(patch, along_axis):
+    near = jnp.sum(lax.all_gather(patch, axis_name=along_axis), 0)
+    return near
+
+
+name_classes = functools.partial(deliver_task, along_axis="tp")
 
 
 def row_rescale(values, gain):
@@ -142,8 +151,8 @@
     head_terms = jnp.dot(mixed_inputs, output_weight, preferred_element_type=jnp.float32)
     own_columns = tokens.shape[1]
     column_start = lax.axis_index("tp") * own_columns
-    residual = present_rows.astype(jnp.float32) + lax.psum(
-        head_terms.astype(jnp.bfloat16), "tp"
+    residual = present_rows.astype(jnp.float32) + name_classes(
+        head_terms.astype(jnp.bfloat16)
     ).astype(jnp.float32)
     expert_rows = row_rescale(residual, second_norm_gain).astype(jnp.bfloat16)
     residual_own = lax.dynamic_slice_in_dim(residual, column_start, own_columns, 1)

time: 154 us -> 131 us (0.85)
  waiting for transfers between devices: 60.5 us -> 28.7 us
  blocking collectives: 33.3 us -> 42.8 us
    psum x1 -> x0, waiting for transfers between devices: 31.7 us -> none  [shards(): lax.psum(head_terms.astype(jnp.bfloat16), 'tp').astype(jnp.float32)]
    all_gather x0 -> x1, blocking collectives: none -> 7.37 us  [deliver_task(): near = jnp.sum(lax.all_gather(patch, axis_name=along_axis), 0)]
  transfers between devices with their start and end apart: 3 -> 2, of which waited for: 3 -> 2; matrix products, arithmetic and copies ran while one was open for 1% -> 0% of each run, Pallas kernels for 0% -> 0%
where the time goes in v1:
time: 131 us
  blocking collectives  42.8 us (33%)
  waiting for transfers between devices  28.7 us (22%)
  matrix products  25.1 us (19%)
  between operations  14.4 us (11%)
  other arithmetic  7.07 us (5%)
  local copies, waits for them, and re-layouts  7.03 us (5%)
  starting transfers between devices  5.55 us (4%)
    reduce_scatter x1, waiting for transfers between devices, shards(): lax.psum_scatter(down_terms.astype(jnp.bfloat16), 'tp', scatter_dimension...  21.3 us
    all_to_all x1, blocking collectives, shards(): lax.all_to_all(outgoing, 'ep', split_axis=0, concat_axis=0, tiled=True)  14.2 us
    all_gather x1, blocking collectives, shards(): lax.all_gather(lax.all_to_all(outgoing, 'ep', split_axis=0, concat_axis=0...  8.58 us
    dot_general x1, matrix products, head_combiner(): along = jnp.einsum('shij,shj->shi', state, removal, precision=highest)  8.53 us
    all_to_all x1, waiting for transfers between devices, shards(): lax.all_to_all(shares, 'ep', split_axis=0, concat_axis=0, tiled=True)  7.37 us
    all_gather x1, blocking collectives, deliver_task(): near = jnp.sum(lax.all_gather(patch, axis_name=along_axis), 0)  7.37 us
    all_gather x1, blocking collectives, shards(): lax.all_gather(tokens, 'tp', axis=1, tiled=True)  6.85 us
    dot_general x1, matrix products, head_combiner(): jnp.einsum('shij,shj->shi', new_state, receptance_rows, precision=highest)  6.58 us
  transfers between devices with their start and end apart: 2, of which 2 were waited for; matrix products, arithmetic and copies ran while one was open for 0% of the time, Pallas kernels for 0%

profile of v1, /device:TPU:0, one launch (start us, length us, event | category | flops | bytes accessed | tf_op | source)
XLA Modules:
  0.0 130.6 jit_solution(6139759820896175238)
XLA Ops:
  7.3 6.9 %all_gather.15 = bf16[32,2048]{1,0:T(8,128)(2,1)S(1)} all-gather(bf16[32,512]{1,0:T(8,128)(2,1)} %param.24), channel_id=1, replica_groups=mesh['ep'=8,'tp'=4] {'tp'}, dimensions={1}, use_global_device_ids=true | all-gather | bytes 163840 | tf_op jit(solution)/shard_map/all_gather | solution.py:125
  14.3 5.8 %all_gather.16 = bf16[32,2048]{1,0:T(8,128)(2,1)S(1)} all-gather(bf16[32,512]{1,0:T(8,128)(2,1)} %param.25), channel_id=1, replica_groups=mesh['ep'=8,'tp'=4] {'tp'}, dimensions={1}, use_global_device_ids=true | all-gather | bytes 163840 | tf_op jit(solution)/shard_map/all_gather | solution.py:126
  20.1 1.1 fusion.83
  21.2 1.6 %fusion.29 = f32[32,256]{1,0:T(8,128)S(1)} fusion(bf16[2048,256]{1,0:T(8,128)(2,1)} %param.28, bf16[32,2048]{1,0:T(8,128)(2,1)S(1)} %all_gather.15, bf16[32,2048]{1,0:T(8,128)(2,1)S(1)} %all_gather.16, f32[2048]{0:T(1024)S(1)} %bitcast.62, f32[2048]{0:T(1024)} %param.26, f32[32]{0:T(128)S(1)} %add_rsqrt_fusion.3), kind=kOutput, calls=%fused_computation.45 | convolution fusion | flops 34078720 | bytes 1360000 | tf_op jit(solution)/shard_map/dot_general | solution.py:55
  22.8 0.7 reshape.161
  23.5 1.4 %fusion.10 = f32[32,256]{1,0:T(8,128)S(1)} fusion(bf16[2048,128]{1,0:T(8,128)(2,1)} %param.34, bf16[32,2048]{1,0:T(8,128)(2,1)S(1)} %all_gather.15, bf16[32,2048]{1,0:T(8,128)(2,1)S(1)} %all_gather.16, f32[2048]{0:T(1024)S(1)} %bitcast.64, f32[2048]{0:T(1024)} %param.26, f32[32]{0:T(128)S(1)} %add_rsqrt_fusion.3, bf16[128,1024]{1,0:T(8,128)(2,1)} %param.35, ...), kind=kOutput, calls=%fused_computation.18 | convolution fusion | flops 19427328 | bytes 901252 | tf_op jit(solution)/shard_map/dot_general | solution.py:55
  25.1 1.6 %fusion.35 = f32[32,256]{1,0:T(8,128)S(1)} fusion(bf16[2048,256]{1,0:T(8,128)(2,1)} %param.29, bf16[32,2048]{1,0:T(8,128)(2,1)S(1)} %all_gather.15, bf16[32,2048]{1,0:T(8,128)(2,1)S(1)} %all_gather.16, f32[2048]{0:T(1024)S(1)} %bitcast.61, f32[2048]{0:T(1024)} %param.26, f32[32]{0:T(128)S(1)} %add_rsqrt_fusion.3), kind=kOutput, calls=%fused_computation.47 | convolution fusion | flops 34078720 | bytes 1360000 | tf_op jit(solution)/shard_map/dot_general | solution.py:55
  27.1 1.3 fusion.67
  28.5 0.3 fusion.31
  29.0 8.5 %fusion.84 = f32[32,4,1,64]{3,2,1,0:T(1,128)S(1)} fusion(f32[32,4,64,1]{2,3,1,0:T(1,128)S(1)} %bitcast.58, f32[32,4,64,64]{3,2,1,0:T(8,128)} %param.41), kind=kOutput, calls=%fused_computation.105 | convolution fusion | flops 6291456 | bytes 2162688 | tf_op jit(solution)/shard_map/shij,shj->shi/dot_general | solution.py:72
  37.5 2.7 %multiply_add_fusion = f32[32,4,64,64]{3,2,1,0:T(8,128)S(1)} fusion(f32[32,4,64,64]{3,2,1,0:T(8,128)S(1)} %copy-done.1, f32[32,4,64]{2,1,0:T(4,128)S(1)} %get-tuple-element.8, f32[32,4,64]{2,1,0:T(4,128)S(1)} %mul.306, f32[32,4,64]{2,1,0:T(4,128)S(1)} %get-tuple-element.4, f32[32,4,64]{2,1,0:T(4,128)S(1)} %bitcast.56, f32[32,4,64]{2,1,0:T(4,128)S(1)} %mul.284), kind=kLoop, calls=%fused_computation.2 | loop fusion | flops 2621440 | bytes 4358144 | tf_op jit(solution)/shard_map/add | solution.py:74
  40.4 2.0 %copy-done.2 = f32[32,4,64,64]{3,2,1,0:T(8,128)} copy-done((f32[32,4,64,64]{3,2,1,0:T(8,128)}, f32[32,4,64,64]{3,2,1,0:T(8,128)S(1)}, u32[]{:S(2)}) %copy-start.2) | copy-done | bytes 2097176
  42.3 6.6 %fusion.85 = f32[32,4,1,64]{3,2,1,0:T(1,128)S(1)} fusion(f32[32,4,64,64]{3,2,1,0:T(8,128)S(1)} %multiply_add_fusion, f32[32,4,64,1]{2,3,1,0:T(1,128)S(1)} %bitcast.57), kind=kOutput, calls=%fused_computation.106 | convolution fusion | flops 6291456 | bytes 2162688 | tf_op jit(solution)/shard_map/shij,shj->shi/dot_general | solution.py:78
  49.0 0.2 multiply_reduce_fusion.2
  49.2 0.6 add_rsqrt_fusion
  49.9 1.4 %fusion.7 = bf16[32,4,64]{2,1,0:T(4,128)(2,1)S(1)} fusion(f32[32,4,64]{2,1,0:T(4,128)S(1)} %mul.306, f32[32,4,64]{2,1,0:T(4,128)S(1)} %bitcast.55, f32[4,64]{1,0:T(4,128)S(1)} %mul.320, f32[32,4]{1,0:T(8,128)} %add_rsqrt_fusion, f32[32,4]{1,0:T(8,128)S(1)} %broadcast_multiply_fusion, f32[32,4,64]{2,1,0:T(4,128)} %reshape.161, ...), kind=kOutput, calls=%fused_computation.14 | output fusion | flops 65727 | bytes 150528 | tf_op jit(solution)/shard_map/mul | solution.py:87
  51.4 0.3 convolution_convert_fusion.1
  51.7 7.4 %all-gather = bf16[128,2048]{1,0:T(8,128)(2,1)S(1)} all-gather(bf16[32,2048]{1,0:T(8,128)(2,1)S(1)} %convolution_convert_fusion.1), channel_id=2, replica_groups=mesh['ep'=8,'tp'=4] {'tp'}, dimensions={0}, use_global_device_ids=true | all-gather | bytes 655360 | tf_op jit(solution)/shard_map/all_gather | solution.py:15
  59.6 0.2 reduce_window_sum.11
  60.3 0.8 dynamic-slice
  61.0 0.2 convolution_convert_fusion.2
  61.3 14.2 %all_to_all.10 = bf16[8,24,512]{2,1,0:T(8,128)(2,1)S(1)} all-to-all(bf16[8,24,512]{2,1,0:T(8,128)(2,1)S(1)} %bitcast.52), channel_id=1, replica_groups=mesh['ep'=8,'tp'=4] {'ep'}, dimensions={0} | all-to-all | bytes 393216 | tf_op jit(solution)/shard_map/all_to_all | solution.py:176
  75.5 8.6 %all_gather.19 = bf16[8,24,2048]{2,1,0:T(8,128)(2,1)S(1)} all-gather(bf16[8,24,512]{2,1,0:T(8,128)(2,1)S(1)} %all_to_all.10), channel_id=1, replica_groups=mesh['ep'=8,'tp'=4] {'tp'}, dimensions={2}, use_global_device_ids=true | all-gather | bytes 983040 | tf_op jit(solution)/shard_map/all_gather | solution.py:175
  84.1 0.4 convolution_minimum_fusion
  84.5 1.6 %fusion.4 = bf16[192,256]{1,0:T(8,128)(2,1)S(1)} fusion(f32[192,256]{1,0:T(8,128)S(1)} %convolution_minimum_fusion, bf16[192,2048]{1,0:T(8,128)(2,1)S(1)} %bitcast.50, bf16[1,2048,256]{2,1,0:T(8,128)(2,1)} %param.46), kind=kOutput, calls=%fused_computation.11 | convolution fusion | flops 201768960 | bytes 2129920 | tf_op jit(solution)/shard_map/dot_general | solution.py:187
  86.1 1.3 convolution_convert_fusion
  87.4 21.3 %reduce-scatter.2.cloned.1.call-done = bf16[8,24,512]{2,1,0:T(8,128)(2,1)} async-done(((bf16[8,24,2048]{2,1,0:T(8,128)(2,1)}), bf16[8,24,512]{2,1,0:T(8,128)(2,1)}) %reduce-scatter.2.cloned.1.call-update) | async-done | bytes 196624 | tf_op jit(solution)/shard_map/reduce_scatter | solution.py:196
  108.7 5.5 %all-to-all-start.1 = ((bf16[8,24,512]{2,1,0:T(8,128)(2,1)}), bf16[8,24,512]{2,1,0:T(8,128)(2,1)S(1)}, u32[]{:S(2)}, u32[]{:S(2)}) async-start(bf16[8,24,512]{2,1,0:T(8,128)(2,1)} %reduce-scatter.2.cloned.1.call-done), calls=%async_computation.2 | async-start | bytes 393216 | tf_op jit(solution)/shard_map/all_to_all | solution.py:199
  114.6 7.4 %all-to-all-done.1 = bf16[8,24,512]{2,1,0:T(8,128)(2,1)S(1)} async-done(((bf16[8,24,512]{2,1,0:T(8,128)(2,1)}), bf16[8,24,512]{2,1,0:T(8,128)(2,1)S(1)}, u32[]{:S(2)}, u32[]{:S(2)}) %all-to-all-start.1) | async-done | bytes 196640 | tf_op jit(solution)/shard_map/all_to_all | solution.py:199
  122.0 0.8 gather_fusion
  122.9 0.3 multiply_reduce_fusion
  123.2 0.6 add_convert_fusion
  (66 shorter events, 2.9 us)
Async XLA Ops:
  7.2 78.9 %copy-start = (bf16[1,256,2048]{2,1,0:T(8,128)(2,1)S(1)}, bf16[1,256,2048]{2,1,0:T(8,128)(2,1)}, u32[]{:S(2)}) copy-start(bf16[1,256,2048]{2,1,0:T(8,128)(2,1)} %param.47) | copy-start | bytes 3145732
  7.2 19.9 %copy-start.6 = (f32[2048]{0:T(1024)S(1)}, f32[2048]{0:T(1024)}, u32[]{:S(2)}) copy-start(f32[2048]{0:T(1024)} %param.26) | copy-start | bytes 24580
  7.2 19.6 %copy-start.9 = (f32[256]{0:T(256)S(1)}, f32[256]{0:T(256)}, u32[]{:S(2)}) copy-start(f32[256]{0:T(256)} %param.36) | copy-start | bytes 3076
  7.2 19.8 %copy-start.10 = (f32[256]{0:T(256)S(1)}, f32[256]{0:T(256)}, u32[]{:S(2)}) copy-start(f32[256]{0:T(256)} %param.37) | copy-start | bytes 3076
  7.2 19.9 %copy-start.12 = (bf16[2048,128]{1,0:T(8,128)(2,1)S(1)}, bf16[2048,128]{1,0:T(8,128)(2,1)}, u32[]{:S(2)}) copy-start(bf16[2048,128]{1,0:T(8,128)(2,1)} %param.31) | copy-start | bytes 1572868
  7.2 19.8 %copy-start.14 = (f32[256]{0:T(256)S(1)}, f32[256]{0:T(256)}, u32[]{:S(2)}) copy-start(f32[256]{0:T(256)} %param.33) | copy-start | bytes 3076
  7.2 21.2 %copy-start.3 = (bf16[2048,256]{1,0:T(8,128)(2,1)S(1)}, bf16[2048,256]{1,0:T(8,128)(2,1)}, u32[]{:S(2)}) copy-start(bf16[2048,256]{1,0:T(8,128)(2,1)} %param.30) | copy-start | bytes 3145732
  7.2 101.5 %reduce-scatter.2.cloned.1.call-start = ((), (), s32[]{:S(2)}) async-start(), calls=%async_computation.3 | async-start | bytes 983040 | tf_op jit(solution)/shard_map/reduce_scatter | solution.py:196
  28.9 8.7 %copy-start.1 = (f32[32,4,64,64]{3,2,1,0:T(8,128)S(1)}, f32[32,4,64,64]{3,2,1,0:T(8,128)}, u32[]{:S(2)}) copy-start(f32[32,4,64,64]{3,2,1,0:T(8,128)} %param.41) | copy-start | bytes 6291460
  40.3 2.0 %copy-start.2 = (f32[32,4,64,64]{3,2,1,0:T(8,128)}, f32[32,4,64,64]{3,2,1,0:T(8,128)S(1)}, u32[]{:S(2)}) copy-start(f32[32,4,64,64]{3,2,1,0:T(8,128)S(1)} %multiply_add_fusion) | copy-start | bytes 6291460
  40.3 9.5 %copy-start.11 = (f32[256]{0:T(256)S(1)}, f32[256]{0:T(256)}, u32[]{:S(2)}) copy-start(f32[256]{0:T(256)} %param.39) | copy-start | bytes 3076
  40.3 9.6 %copy-start.13 = (f32[4,64]{1,0:T(4,128)S(1)}, f32[4,64]{1,0:T(4,128)}, u32[]{:S(2)}) copy-start(f32[4,64]{1,0:T(4,128)} %param.38) | copy-start | bytes 3076
  40.3 11.1 %copy-start.4 = (bf16[256,2048]{1,0:T(8,128)(2,1)S(1)}, bf16[256,2048]{1,0:T(8,128)(2,1)}, u32[]{:S(2)}) copy-start(bf16[256,2048]{1,0:T(8,128)(2,1)} %param.40) | copy-start | bytes 3145732
  40.3 19.0 %copy-start.7 = (s32[32,4]{0,1:T(4,128)S(1)}, s32[32,4]{0,1:T(4,128)}, u32[]{:S(2)}) copy-start(s32[32,4]{0,1:T(4,128)} %param.43) | copy-start | bytes 1540
  42.3 41.8 %copy-start.5 = (bf16[1,2048,256]{2,1,0:T(8,128)(2,1)S(1)}, bf16[1,2048,256]{2,1,0:T(8,128)(2,1)}, u32[]{:S(2)}) copy-start(bf16[1,2048,256]{2,1,0:T(8,128)(2,1)} %param.45) | copy-start | bytes 3145732
  84.1 30.5 %copy-start.8 = (f32[32,4]{0,1:T(4,128)S(1)}, f32[32,4]{0,1:T(4,128)}, u32[]{:S(2)}) copy-start(f32[32,4]{0,1:T(4,128)} %param.44) | copy-start | bytes 1540
  108.7 13.3 %all-to-all-start.1 = ((bf16[8,24,512]{2,1,0:T(8,128)(2,1)}), bf16[8,24,512]{2,1,0:T(8,128)(2,1)S(1)}, u32[]{:S(2)}, u32[]{:S(2)}) async-start(bf16[8,24,512]{2,1,0:T(8,128)(2,1)} %reduce-scatter.2.cloned.1.call-done), calls=%async_computation.2 | async-start | bytes 393216 | tf_op jit(solution)/shard_map/all_to_all | solution.py:199
Sparse Core Ops, SparseCore 0:
  87.5 21.1 reduce-scatter.1
